TPU v7x, 32 devices: a whole 2x2x4 slice. The times are simulated.
32 devices in a mesh: grp: 2 (over y), fs: 4 (over z), tp: 4 (over x, core).
Axes of the slice: x: 2, y: 2, z: 4, core: 2. Of those that a mesh axis runs over, the one named last changes fastest.
Arguments:
- tokens: bfloat16 [32, 128, 2048], P(('grp', 'fs'), None, 'tp'), parts along dimension 0, may hold values from -100 to 100
- mix_gain: float32 [2048], replicated, may hold values from 0.1 to 1.9
- gate_outer: bfloat16 [2048, 1024], P('fs', 'tp'), may hold values from -0.125 to 0.125
- gate_inner: bfloat16 [2048, 1024], P('fs', 'tp'), may hold values from -0.125 to 0.125
- value_weight: bfloat16 [2048, 1024], P('fs', 'tp'), may hold values from -0.125 to 0.125
- conv_taps: float32 [3, 1024], replicated, may hold values from -3 to 3
- mix_out: bfloat16 [1024, 2048], P('tp', 'fs'), may hold values from -0.25 to 0.25
- ffn_gain: float32 [2048], replicated, may hold values from 0.1 to 1.9
- ffn_gate: bfloat16 [2048, 5632], P('fs', 'tp'), may hold values from -0.125 to 0.125
- ffn_up: bfloat16 [2048, 5632], P('fs', 'tp'), may hold values from -0.125 to 0.125
- ffn_down: bfloat16 [5632, 2048], P('tp', 'fs'), may hold values from -0.109375 to 0.109375
- out_gain: float32 [2048], replicated, may hold values from 0.1 to 1.9
Outputs:
- layer_out: bfloat16 [32, 128, 2048], P(('grp', 'fs'), None, 'tp'), parts along dimension 0
There are 2 independent parts, one for each index of `grp`. A program takes and returns all parts, laid end to end along the dimension named above; an argument that names none is the same for every part. Nothing has to cross between parts.
All inputs are finite; a program needn't handle non-finite values.
Results may differ from a plain program's by a relative error of at most 0.015.
Values may be sent and summed in bfloat16 or wider, within the bound.
A program may use at most 64 MiB of HBM per device.

v0:
```python
import jax
import jax.numpy as jnp
from jax import lax
from jax.sharding import PartitionSpec as P


def rms_norm(values, gain):
    floats = values.astype(jnp.float32)
    scaled = floats * lax.rsqrt(jnp.mean(floats * floats, axis=-1, keepdims=True) + 1e-06)
    return (scaled * gain).astype(jnp.bfloat16)


def local(
    tokens,
    mix_gain,
    gate_outer,
    gate_inner,
    value_weight,
    conv_taps,
    mix_out,
    ffn_gain,
    ffn_gate,
    ffn_up,
    ffn_down,
    out_gain,
):
    seq_count, length, columns = tokens.shape
    row_count = seq_count * length
    width = columns * lax.axis_size("tp")
    whole = lax.all_gather(tokens, "tp", axis=2, tiled=True).reshape(row_count, width)
    normed = rms_norm(whole, mix_gain)
    channels = gate_outer.shape[1]
    pieces = (
        lax.all_gather(gate_outer, "fs", axis=0, tiled=True),
        lax.all_gather(gate_inner, "fs", axis=0, tiled=True),
        lax.all_gather(value_weight, "fs", axis=0, tiled=True),
    )
    sliced = normed
    outer = jnp.dot(sliced, pieces[0], preferred_element_type=jnp.float32)
    inner = jnp.dot(sliced, pieces[1], preferred_element_type=jnp.float32)
    values = jnp.dot(sliced, pieces[2], preferred_element_type=jnp.float32)
    outer = outer.astype(jnp.bfloat16)
    inner = inner.astype(jnp.bfloat16)
    values = values.astype(jnp.bfloat16)
    product = (inner.astype(jnp.float32) * values.astype(jnp.float32)).reshape(
        seq_count, length, channels
    )
    own_taps = lax.dynamic_slice_in_dim(conv_taps, lax.axis_index("tp") * channels, channels, 1)
    tap_count = conv_taps.shape[0]
    padded = jnp.pad(product, ((0, 0), (tap_count - 1, 0), (0, 0)))
    conv = jnp.zeros((seq_count, length, channels), jnp.float32)
    for offset in range(tap_count):
        conv = conv + own_taps[offset] * padded[:, offset : offset + length]
    gated = (outer.astype(jnp.float32) * conv.reshape(row_count, channels)).astype(jnp.bfloat16)
    mix_terms = jnp.dot(
        gated, lax.all_gather(mix_out, "fs", axis=1, tiled=True), preferred_element_type=jnp.float32
    )
    mix_full = lax.psum(mix_terms.astype(jnp.bfloat16), "tp").astype(jnp.float32)
    first_full = (whole.astype(jnp.float32) + mix_full).astype(jnp.bfloat16)
    first = lax.dynamic_slice_in_dim(first_full, lax.axis_index("tp") * columns, columns, 1)
    normed_ffn = rms_norm(first_full, ffn_gain)
    pieces = (
        lax.all_gather(ffn_gate, "fs", axis=0, tiled=True),
        lax.all_gather(ffn_up, "fs", axis=0, tiled=True),
    )
    sliced = normed_ffn
    gate = jnp.dot(sliced, pieces[0], preferred_element_type=jnp.float32)
    upward = jnp.dot(sliced, pieces[1], preferred_element_type=jnp.float32)
    hidden = (jax.nn.silu(gate) * upward).astype(jnp.bfloat16)
    down_terms = jnp.dot(
        hidden,
        lax.all_gather(ffn_down, "fs", axis=1, tiled=True),
        preferred_element_type=jnp.float32,
    )
    down_summed = lax.psum_scatter(
        down_terms.astype(jnp.bfloat16), "tp", scatter_dimension=1, tiled=True
    ).astype(jnp.float32)
    second = first.astype(jnp.float32) + down_summed
    squares = lax.psum(jnp.sum(second * second, axis=1), "tp")
    factor = lax.rsqrt(squares / width + 1e-06)
    own_gain = lax.dynamic_slice_in_dim(out_gain, lax.axis_index("tp") * columns, columns, 0)
    result = second * factor[:, None] * own_gain
    return result.astype(jnp.bfloat16).reshape(seq_count, length, columns)


def solution(mesh):
    in_specs = (
        P(("grp", "fs"), None, "tp"),
        P(),
        P("fs", "tp"),
        P("fs", "tp"),
        P("fs", "tp"),
        P(),
        P("tp", "fs"),
        P(),
        P("fs", "tp"),
        P("fs", "tp"),
        P("tp", "fs"),
        P(),
    )
    out_specs = P(("grp", "fs"), None, "tp")
    return jax.shard_map(local, mesh=mesh, in_specs=in_specs, out_specs=out_specs, check_vma=False)
```

profile of v0, /device:TPU:0, one launch (start us, length us, event | category | flops | bytes accessed | tf_op | source)
XLA Modules:
  0.0 587.0 jit_solution(15794149463791373341)
XLA Ops:
  6.5 0.0 copy-start.3
  6.5 0.0 all-gather.9.cloned.1.call-start
  6.5 0.7 all-gather.9.cloned.1.call-update
  7.3 0.0 all-gather.15.cloned.1.call-start
  7.3 0.7 all-gather.15.cloned.1.call-update
  8.0 0.0 all-gather.13.cloned.1.call-start
  8.1 0.7 all-gather.13.cloned.1.call-update
  8.7 0.0 all-gather.11.cloned.1.call-start
  8.8 0.5 all-gather.11.cloned.1.call-update
  9.3 0.0 all-gather.17.cloned.1.call-start
  9.4 0.5 all-gather.17.cloned.1.call-update
  9.9 0.0 all-reduce.3.cloned.1.call-start
  10.0 0.9 constant_dynamic-slice_fusion
  10.8 23.4 %all-gather.9.cloned.1.call-done = bf16[4,128,2048]{2,1,0:T(8,128)(2,1)} async-done(((bf16[4,128,512]{2,1,0:T(8,128)(2,1)}), bf16[4,128,2048]{2,1,0:T(8,128)(2,1)}) %all-gather.9.cloned.1.call-update) | async-done | bytes 2097168 | tf_op jit(solution)/shard_map/all_gather | solution.py:30
  34.2 0.0 copy-start
  34.2 2.2 fusion.3
  36.4 0.0 copy-done.3
  36.5 0.0 copy-done
  36.5 0.5 fusion.5
  37.0 26.8 %all-gather.15.cloned.1.call-done = bf16[2048,256]{1,0:T(8,128)(2,1)} async-done(((bf16[512,256]{1,0:T(8,128)(2,1)}), bf16[2048,256]{1,0:T(8,128)(2,1)}) %all-gather.15.cloned.1.call-update) | async-done | bytes 1048592 | tf_op jit(solution)/shard_map/all_gather | solution.py:36
  63.8 1.9 fusion.13
  65.7 27.0 %all-gather.13.cloned.1.call-done = bf16[2048,256]{1,0:T(8,128)(2,1)} async-done(((bf16[512,256]{1,0:T(8,128)(2,1)}), bf16[2048,256]{1,0:T(8,128)(2,1)}) %all-gather.13.cloned.1.call-update) | async-done | bytes 1048592 | tf_op jit(solution)/shard_map/all_gather | solution.py:35
  92.8 1.9 fusion.12
  94.7 0.2 fusion.20
  94.9 26.7 %all-gather.11.cloned.1.call-done = bf16[2048,256]{1,0:T(8,128)(2,1)} async-done(((bf16[512,256]{1,0:T(8,128)(2,1)}), bf16[2048,256]{1,0:T(8,128)(2,1)}) %all-gather.11.cloned.1.call-update) | async-done | bytes 1048592 | tf_op jit(solution)/shard_map/all_gather | solution.py:34
  121.6 28.8 %all-gather.17.cloned.1.call-done = bf16[256,2048]{1,0:T(8,128)(2,1)} async-done(((bf16[256,512]{1,0:T(8,128)(2,1)}), bf16[256,2048]{1,0:T(8,128)(2,1)}) %all-gather.17.cloned.1.call-update) | async-done | bytes 1048592 | tf_op jit(solution)/shard_map/all_gather | solution.py:56
  150.4 5.2 convolution_convert_fusion
  155.6 0.0 copy-start.1
  155.6 0.0 all-reduce.3.cloned.1.call-update
  155.6 0.0 all-gather.19.cloned.1.call-start
  155.7 0.7 all-gather.19.cloned.1.call-update
  156.4 0.0 all-gather.21.cloned.1.call-start
  156.4 0.7 all-gather.21.cloned.1.call-update
  157.1 0.0 all-gather.23.cloned.1.call-start
  157.2 0.7 all-gather.23.cloned.1.call-update
  157.9 0.0 copy-start.4
  157.9 0.2 reduce-scatter.2.cloned.1.call-start
  158.1 48.4 %all-reduce.3.cloned.1.call-done = bf16[512,2048]{1,0:T(8,128)(2,1)} async-done(((bf16[512,2048]{1,0:T(8,128)(2,1)}), bf16[512,2048]{1,0:T(8,128)(2,1)}) %all-reduce.3.cloned.1.call-update) | async-done | bytes 2097168 | tf_op jit(solution)/shard_map/psum | solution.py:58
  206.5 0.0 copy-done.1
  206.5 3.9 fusion
  210.5 104.4 %all-gather.19.cloned.1.call-done = bf16[2048,1408]{1,0:T(8,128)(2,1)} async-done(((bf16[512,1408]{1,0:T(8,128)(2,1)}), bf16[2048,1408]{1,0:T(8,128)(2,1)}) %all-gather.19.cloned.1.call-update) | async-done | bytes 5767184 | tf_op jit(solution)/shard_map/all_gather | solution.py:63
  314.9 0.0 copy-done.4
  314.9 0.0 copy-start.2
  314.9 8.4 %fusion.16 = f32[512,1408]{1,0:T(8,128)} fusion(bf16[2048,1408]{1,0:T(8,128)(2,1)} %all-gather.19.cloned.1.call-done, bf16[512,2048]{1,0:T(8,128)(2,1)} %get-tuple-element.6, f32[2048]{0:T(1024)S(1)} %copy-done.4, f32[512]{0:T(512)S(1)} %add_rsqrt_fusion.1), kind=kOutput, calls=%fused_computation.28 | convolution fusion | flops 2956984320 | bytes 10758144 | tf_op jit(solution)/shard_map/dot_general | solution.py:67
  323.3 98.1 %all-gather.21.cloned.1.call-done = bf16[2048,1408]{1,0:T(8,128)(2,1)} async-done(((bf16[512,1408]{1,0:T(8,128)(2,1)}), bf16[2048,1408]{1,0:T(8,128)(2,1)}) %all-gather.21.cloned.1.call-update) | async-done | bytes 5767184 | tf_op jit(solution)/shard_map/all_gather | solution.py:64
  421.4 106.5 %all-gather.23.cloned.1.call-done = bf16[1408,2048]{1,0:T(8,128)(2,1)} async-done(((bf16[1408,512]{1,0:T(8,128)(2,1)}), bf16[1408,2048]{1,0:T(8,128)(2,1)}) %all-gather.23.cloned.1.call-update) | async-done | bytes 5767184 | tf_op jit(solution)/shard_map/all_gather | solution.py:72
  528.0 0.0 copy-done.2
  528.0 13.4 %convolution_convert_fusion.1 = bf16[512,2048]{1,0:T(8,128)(2,1)} fusion(bf16[1408,2048]{1,0:T(8,128)(2,1)} %all-gather.23.cloned.1.call-done, bf16[2048,1408]{1,0:T(8,128)(2,1)} %all-gather.21.cloned.1.call-done, f32[512,1408]{1,0:T(8,128)} %fusion.16, bf16[512,2048]{1,0:T(8,128)(2,1)S(1)} %copy-done.2, f32[2048]{0:T(1024)S(1)} %copy-done.4, ...), kind=kOutput, calls=%fused_computation.15 | convolution fusion | flops 5915148288 | bytes 18622464 | tf_op jit(solution)/shard_map/dot_general | solution.py:70
  541.4 0.0 reduce-scatter.2.cloned.1.call-update
  541.4 0.8 dynamic_slice.11
  542.2 28.8 %reduce-scatter.2.cloned.1.call-done = bf16[512,512]{1,0:T(8,128)(2,1)} async-done(((bf16[512,2048]{1,0:T(8,128)(2,1)}), bf16[512,512]{1,0:T(8,128)(2,1)}) %reduce-scatter.2.cloned.1.call-update) | async-done | bytes 524304 | tf_op jit(solution)/shard_map/reduce_scatter | solution.py:75
  571.0 1.3 multiply_reduce_fusion
  572.3 5.8 psum.15
  578.1 2.0 multiply_convert_fusion
  (3 shorter events, 0.0 us)
Async XLA Ops:
  6.5 29.9 %copy-start.3 = (f32[2048]{0:T(1024)S(1)}, f32[2048]{0:T(1024)}, u32[]{:S(2)}) copy-start(f32[2048]{0:T(1024)} %param.13) | copy-start | bytes 24580
  6.5 27.7 %all-gather.9.cloned.1.call-start = ((), (), s32[]{:S(2)}) async-start(), calls=%async_computation.1 | async-start | bytes 2621440 | tf_op jit(solution)/shard_map/all_gather | solution.py:30
  7.3 56.5 %all-gather.15.cloned.1.call-start = ((), (), s32[]{:S(2)}) async-start(), calls=%async_computation.4 | async-start | bytes 1310720 | tf_op jit(solution)/shard_map/all_gather | solution.py:36
  8.0 84.8 %all-gather.13.cloned.1.call-start = ((), (), s32[]{:S(2)}) async-start(), calls=%async_computation.3 | async-start | bytes 1310720 | tf_op jit(solution)/shard_map/all_gather | solution.py:35
  8.7 112.8 %all-gather.11.cloned.1.call-start = ((), (), s32[]{:S(2)}) async-start(), calls=%async_computation.2 | async-start | bytes 1310720 | tf_op jit(solution)/shard_map/all_gather | solution.py:34
  9.3 141.1 %all-gather.17.cloned.1.call-start = ((), (), s32[]{:S(2)}) async-start(), calls=%async_computation.5 | async-start | bytes 1310720 | tf_op jit(solution)/shard_map/all_gather | solution.py:56
  9.9 196.6 %all-reduce.3.cloned.1.call-start = ((), (), s32[]{:S(2)}) async-start(), calls=%async_computation.6 | async-start | bytes 4194304 | tf_op jit(solution)/shard_map/psum | solution.py:58
  34.2 2.2 copy-start
  155.6 50.9 %copy-start.1 = (bf16[4,128,2048]{2,1,0:T(8,128)(2,1)S(1)}, bf16[4,128,2048]{2,1,0:T(8,128)(2,1)}, u32[]{:S(2)}) copy-start(bf16[4,128,2048]{2,1,0:T(8,128)(2,1)} %all-gather.9.cloned.1.call-done) | copy-start | bytes 6291460
  155.6 159.3 %all-gather.19.cloned.1.call-start = ((), (), s32[]{:S(2)}) async-start(), calls=%async_computation.7 | async-start | bytes 7208960 | tf_op jit(solution)/shard_map/all_gather | solution.py:63
  156.4 265.1 %all-gather.21.cloned.1.call-start = ((), (), s32[]{:S(2)}) async-start(), calls=%async_computation.8 | async-start | bytes 7208960 | tf_op jit(solution)/shard_map/all_gather | solution.py:64
  157.1 370.9 %all-gather.23.cloned.1.call-start = ((), (), s32[]{:S(2)}) async-start(), calls=%async_computation.9 | async-start | bytes 7208960 | tf_op jit(solution)/shard_map/all_gather | solution.py:72
  157.9 157.0 %copy-start.4 = (f32[2048]{0:T(1024)S(1)}, f32[2048]{0:T(1024)}, u32[]{:S(2)}) copy-start(f32[2048]{0:T(1024)} %param.19) | copy-start | bytes 24580
  157.9 413.2 %reduce-scatter.2.cloned.1.call-start = ((), (), s32[]{:S(2)}) async-start(), calls=%async_computation.10 | async-start | bytes 2621440 | tf_op jit(solution)/shard_map/reduce_scatter | solution.py:75
  314.9 213.1 %copy-start.2 = (bf16[512,2048]{1,0:T(8,128)(2,1)S(1)}, bf16[512,2048]{1,0:T(8,128)(2,1)}, u32[]{:S(2)}) copy-start(bf16[512,2048]{1,0:T(8,128)(2,1)} %get-tuple-element.6) | copy-start | bytes 6291460
Sparse Core Ops, SparseCore 0:
  8.9 25.2 all-gather.8
  35.8 27.9 all-gather.14
  65.4 27.3 all-gather.12
  94.2 27.3 all-gather.10
  123.0 27.3 all-gather.16
  155.7 50.7 all-reduce.2
  208.1 106.7 all-gather.18
  316.5 104.9 all-gather.20
  423.0 104.9 all-gather.22
  541.6 29.4 reduce-scatter.1
where the time goes:
time: 587 us
  waiting for transfers between devices  524 us (89%)
  matrix products  30.9 us (5%)
  between operations  13.6 us (2%)
  other arithmetic  10.2 us (2%)
    all_gather x1, waiting for transfers between devices, local(): lax.all_gather(ffn_down, 'fs', axis=1, tiled=True)  107 us
    all_gather x1, waiting for transfers between devices, local(): lax.all_gather(ffn_gate, 'fs', axis=0, tiled=True)  104 us
    all_gather x1, waiting for transfers between devices, local(): lax.all_gather(ffn_up, 'fs', axis=0, tiled=True)  98.1 us
    psum x1, waiting for transfers between devices, local(): lax.psum(mix_terms.astype(jnp.bfloat16), 'tp').astype(jnp.float32)  48.4 us
    reduce_scatter x1, waiting for transfers between devices, local(): lax.psum_scatter(down_terms.astype(jnp.bfloat16), 'tp', scatter_dimension...  28.8 us
    all_gather x1, waiting for transfers between devices, local(): lax.all_gather(mix_out, 'fs', axis=1, tiled=True)  28.8 us
    all_gather x1, waiting for transfers between devices, local(): lax.all_gather(gate_inner, 'fs', axis=0, tiled=True)  27 us
    all_gather x1, waiting for transfers between devices, local(): lax.all_gather(value_weight, 'fs', axis=0, tiled=True)  26.8 us
  transfers between devices with their start and end apart: 10, of which 10 were waited for; matrix products, arithmetic and copies ran while one was open for 4% of the time, Pallas kernels for 0%

commit v1 on v0

--- a/solution.py
+++ b/solution.py
@@ -69,7 +69,7 @@
     hidden = (jax.nn.silu(gate) * upward).astype(jnp.bfloat16)
     down_terms = jnp.dot(
         hidden,
-        lax.all_gather(ffn_down, "fs", axis=1, tiled=True),
+        jnp.concatenate(lax.all_gather(ffn_down, "fs"), axis=1),
         preferred_element_type=jnp.float32,
     )
     down_summed = lax.psum_scatter(

time: 587 us -> 587 us (level)
  local copies, waits for them, and re-layouts: 1.66 us -> 10.2 us
  waiting for transfers between devices: 524 us -> 516 us
    reshape x0 -> x1, local copies, waits for them, and re-layouts: none -> 8.51 us  [local(): jnp.concatenate(lax.all_gather(ffn_down, 'fs'), axis=1)]
    all_gather x1, waiting for transfers between devices: 104 us -> 98 us  [local(): lax.all_gather(ffn_gate, 'fs', axis=0, tiled=True)]
  transfers between devices with their start and end apart: 10 -> 10, of which waited for: 10 -> 10; matrix products, arithmetic and copies ran while one was open for 4% -> 5% of each run, Pallas kernels for 0% -> 0%
where the time goes in v1:
time: 587 us
  waiting for transfers between devices  516 us (88%)
  matrix products  30.1 us (5%)
  between operations  13.6 us (2%)
  local copies, waits for them, and re-layouts  10.2 us (2%)
  other arithmetic  10.2 us (2%)
    all_gather x1, waiting for transfers between devices, local(): lax.all_gather(ffn_down, 'fs')  104 us
    all_gather x1, waiting for transfers between devices, local(): lax.all_gather(ffn_up, 'fs', axis=0, tiled=True)  98.8 us
    all_gather x1, waiting for transfers between devices, local(): lax.all_gather(ffn_gate, 'fs', axis=0, tiled=True)  98 us
    psum x1, waiting for transfers between devices, local(): lax.psum(mix_terms.astype(jnp.bfloat16), 'tp').astype(jnp.float32)  48.4 us
    reduce_scatter x1, waiting for transfers between devices, local(): lax.psum_scatter(down_terms.astype(jnp.bfloat16), 'tp', scatter_dimension...  28.8 us
    all_gather x1, waiting for transfers between devices, local(): lax.all_gather(mix_out, 'fs', axis=1, tiled=True)  28.8 us
    all_gather x1, waiting for transfers between devices, local(): lax.all_gather(gate_inner, 'fs', axis=0, tiled=True)  27 us
    all_gather x1, waiting for transfers between devices, local(): lax.all_gather(value_weight, 'fs', axis=0, tiled=True)  26.8 us
  transfers between devices with their start and end apart: 10, of which 10 were waited for; matrix products, arithmetic and copies ran while one was open for 5% of the time, Pallas kernels for 0%

profile of v1, /device:TPU:0, one launch (start us, length us, event | category | flops | bytes accessed | tf_op | source)
XLA Modules:
  0.0 586.8 jit_solution(5077442243285369977)
XLA Ops:
  6.5 0.0 copy-start.3
  6.5 0.0 all-gather.10.cloned.1.call-start
  6.5 0.7 all-gather.10.cloned.1.call-update
  7.3 0.0 all-gather.16.cloned.1.call-start
  7.3 0.7 all-gather.16.cloned.1.call-update
  8.0 0.0 all-gather.14.cloned.1.call-start
  8.1 0.7 all-gather.14.cloned.1.call-update
  8.7 0.0 all-gather.12.cloned.1.call-start
  8.8 0.5 all-gather.12.cloned.1.call-update
  9.3 0.0 all-gather.18.cloned.1.call-start
  9.4 0.5 all-gather.18.cloned.1.call-update
  9.9 0.0 all-reduce.3.cloned.1.call-start
  10.0 0.9 constant_dynamic-slice_fusion
  10.8 23.4 %all-gather.10.cloned.1.call-done = bf16[4,128,2048]{2,1,0:T(8,128)(2,1)} async-done(((bf16[4,128,512]{2,1,0:T(8,128)(2,1)}), bf16[4,128,2048]{2,1,0:T(8,128)(2,1)}) %all-gather.10.cloned.1.call-update) | async-done | bytes 2097168 | tf_op jit(solution)/shard_map/all_gather | solution.py:30
  34.2 0.0 copy-start
  34.2 2.2 fusion.3
  36.4 0.0 copy-done.3
  36.5 0.0 copy-done
  36.5 0.5 fusion.5
  37.0 26.8 %all-gather.16.cloned.1.call-done = bf16[2048,256]{1,0:T(8,128)(2,1)} async-done(((bf16[512,256]{1,0:T(8,128)(2,1)}), bf16[2048,256]{1,0:T(8,128)(2,1)}) %all-gather.16.cloned.1.call-update) | async-done | bytes 1048592 | tf_op jit(solution)/shard_map/all_gather | solution.py:36
  63.8 1.9 fusion.13
  65.7 27.0 %all-gather.14.cloned.1.call-done = bf16[2048,256]{1,0:T(8,128)(2,1)} async-done(((bf16[512,256]{1,0:T(8,128)(2,1)}), bf16[2048,256]{1,0:T(8,128)(2,1)}) %all-gather.14.cloned.1.call-update) | async-done | bytes 1048592 | tf_op jit(solution)/shard_map/all_gather | solution.py:35
  92.8 1.9 fusion.12
  94.7 0.2 fusion.20
  94.9 26.7 %all-gather.12.cloned.1.call-done = bf16[2048,256]{1,0:T(8,128)(2,1)} async-done(((bf16[512,256]{1,0:T(8,128)(2,1)}), bf16[2048,256]{1,0:T(8,128)(2,1)}) %all-gather.12.cloned.1.call-update) | async-done | bytes 1048592 | tf_op jit(solution)/shard_map/all_gather | solution.py:34
  121.6 28.8 %all-gather.18.cloned.1.call-done = bf16[256,2048]{1,0:T(8,128)(2,1)} async-done(((bf16[256,512]{1,0:T(8,128)(2,1)}), bf16[256,2048]{1,0:T(8,128)(2,1)}) %all-gather.18.cloned.1.call-update) | async-done | bytes 1048592 | tf_op jit(solution)/shard_map/all_gather | solution.py:56
  150.4 5.2 convolution_convert_fusion
  155.6 0.0 copy-start.1
  155.6 0.0 all-reduce.3.cloned.1.call-update
  155.6 0.0 all-gather.24.cloned.1.call-start
  155.7 0.7 all-gather.24.cloned.1.call-update
  156.4 0.0 all-gather.20.cloned.1.call-start
  156.4 0.7 all-gather.20.cloned.1.call-update
  157.1 0.0 all-gather.22.cloned.1.call-start
  157.2 0.7 all-gather.22.cloned.1.call-update
  157.9 0.2 reduce-scatter.2.cloned.1.call-start
  158.1 48.4 %all-reduce.3.cloned.1.call-done = bf16[512,2048]{1,0:T(8,128)(2,1)} async-done(((bf16[512,2048]{1,0:T(8,128)(2,1)}), bf16[512,2048]{1,0:T(8,128)(2,1)}) %all-reduce.3.cloned.1.call-update) | async-done | bytes 2097168 | tf_op jit(solution)/shard_map/psum | solution.py:58
  206.5 0.0 copy-done.1
  206.5 3.9 fusion
  210.5 104.4 %all-gather.24.cloned.1.call-done = bf16[5632,512]{1,0:T(8,128)(2,1)} async-done(((bf16[1408,512]{1,0:T(8,128)(2,1)}), bf16[5632,512]{1,0:T(8,128)(2,1)}) %all-gather.24.cloned.1.call-update) | async-done | bytes 5767184 | tf_op jit(solution)/shard_map/all_gather | solution.py:72
  314.9 0.0 copy-start.2
  314.9 0.0 copy-start.4
  314.9 8.5 %copy.13 = bf16[1408,4,512]{0,2,1:T(8,128)(2,1)} copy(bf16[1408,4,512]{2,0,1:T(8,128)(2,1)} %bitcast.32) | data formatting | bytes 11534336 | tf_op jit(solution)/shard_map/reshape | solution.py:72
  323.4 98.0 %all-gather.20.cloned.1.call-done = bf16[2048,1408]{1,0:T(8,128)(2,1)} async-done(((bf16[512,1408]{1,0:T(8,128)(2,1)}), bf16[2048,1408]{1,0:T(8,128)(2,1)}) %all-gather.20.cloned.1.call-update) | async-done | bytes 5767184 | tf_op jit(solution)/shard_map/all_gather | solution.py:63
  421.4 0.0 copy-done.2
  421.4 0.0 copy-done.4
  421.5 7.7 %fusion.16 = f32[512,1408]{1,0:T(8,128)} fusion(bf16[2048,1408]{1,0:T(8,128)(2,1)} %all-gather.20.cloned.1.call-done, bf16[512,2048]{1,0:T(8,128)(2,1)S(1)} %copy-done.2, f32[2048]{0:T(1024)S(1)} %copy-done.4, f32[512]{0:T(512)S(1)} %add_rsqrt_fusion.1), kind=kOutput, calls=%fused_computation.28 | convolution fusion | flops 2956984320 | bytes 10758144 | tf_op jit(solution)/shard_map/dot_general | solution.py:67
  429.2 98.8 %all-gather.22.cloned.1.call-done = bf16[2048,1408]{1,0:T(8,128)(2,1)} async-done(((bf16[512,1408]{1,0:T(8,128)(2,1)}), bf16[2048,1408]{1,0:T(8,128)(2,1)}) %all-gather.22.cloned.1.call-update) | async-done | bytes 5767184 | tf_op jit(solution)/shard_map/all_gather | solution.py:64
  528.0 13.3 %convolution_convert_fusion.1 = bf16[512,2048]{1,0:T(8,128)(2,1)} fusion(bf16[1408,2048]{0,1:T(8,128)(2,1)} %bitcast.33, bf16[2048,1408]{1,0:T(8,128)(2,1)} %all-gather.22.cloned.1.call-done, f32[512,1408]{1,0:T(8,128)} %fusion.16, bf16[512,2048]{1,0:T(8,128)(2,1)S(1)} %copy-done.2, f32[2048]{0:T(1024)S(1)} %copy-done.4, f32[512]{0:T(512)S(1)} %add_rsqrt_fusion.1), kind=kOutput, calls=%fused_computation.15 | convolution fusion | flops 5915148288 | bytes 18622464 | tf_op jit(solution)/shard_map/dot_general | solution.py:70
  541.3 0.0 reduce-scatter.2.cloned.1.call-update
  541.3 0.8 dynamic_slice.11
  542.0 28.8 %reduce-scatter.2.cloned.1.call-done = bf16[512,512]{1,0:T(8,128)(2,1)} async-done(((bf16[512,2048]{1,0:T(8,128)(2,1)}), bf16[512,512]{1,0:T(8,128)(2,1)}) %reduce-scatter.2.cloned.1.call-update) | async-done | bytes 524304 | tf_op jit(solution)/shard_map/reduce_scatter | solution.py:75
  570.9 1.3 multiply_reduce_fusion
  572.2 5.8 psum.15
  577.9 2.0 multiply_convert_fusion
  (3 shorter events, 0.0 us)
Async XLA Ops:
  6.5 29.9 %copy-start.3 = (f32[2048]{0:T(1024)S(1)}, f32[2048]{0:T(1024)}, u32[]{:S(2)}) copy-start(f32[2048]{0:T(1024)} %param.13) | copy-start | bytes 24580
  6.5 27.7 %all-gather.10.cloned.1.call-start = ((), (), s32[]{:S(2)}) async-start(), calls=%async_computation.1 | async-start | bytes 2621440 | tf_op jit(solution)/shard_map/all_gather | solution.py:30
  7.3 56.5 %all-gather.16.cloned.1.call-start = ((), (), s32[]{:S(2)}) async-start(), calls=%async_computation.4 | async-start | bytes 1310720 | tf_op jit(solution)/shard_map/all_gather | solution.py:36
  8.0 84.8 %all-gather.14.cloned.1.call-start = ((), (), s32[]{:S(2)}) async-start(), calls=%async_computation.3 | async-start | bytes 1310720 | tf_op jit(solution)/shard_map/all_gather | solution.py:35
  8.7 112.8 %all-gather.12.cloned.1.call-start = ((), (), s32[]{:S(2)}) async-start(), calls=%async_computation.2 | async-start | bytes 1310720 | tf_op jit(solution)/shard_map/all_gather | solution.py:34
  9.3 141.1 %all-gather.18.cloned.1.call-start = ((), (), s32[]{:S(2)}) async-start(), calls=%async_computation.5 | async-start | bytes 1310720 | tf_op jit(solution)/shard_map/all_gather | solution.py:56
  9.9 196.6 %all-reduce.3.cloned.1.call-start = ((), (), s32[]{:S(2)}) async-start(), calls=%async_computation.6 | async-start | bytes 4194304 | tf_op jit(solution)/shard_map/psum | solution.py:58
  34.2 2.2 copy-start
  155.6 50.9 %copy-start.1 = (bf16[4,128,2048]{2,1,0:T(8,128)(2,1)S(1)}, bf16[4,128,2048]{2,1,0:T(8,128)(2,1)}, u32[]{:S(2)}) copy-start(bf16[4,128,2048]{2,1,0:T(8,128)(2,1)} %all-gather.10.cloned.1.call-done) | copy-start | bytes 6291460
  155.6 159.3 %all-gather.24.cloned.1.call-start = ((), (), s32[]{:S(2)}) async-start(), calls=%async_computation.10 | async-start | bytes 7208960 | tf_op jit(solution)/shard_map/all_gather | solution.py:72
  156.4 265.1 %all-gather.20.cloned.1.call-start = ((), (), s32[]{:S(2)}) async-start(), calls=%async_computation.7 | async-start | bytes 7208960 | tf_op jit(solution)/shard_map/all_gather | solution.py:63
  157.1 370.9 %all-gather.22.cloned.1.call-start = ((), (), s32[]{:S(2)}) async-start(), calls=%async_computation.8 | async-start | bytes 7208960 | tf_op jit(solution)/shard_map/all_gather | solution.py:64
  157.9 413.0 %reduce-scatter.2.cloned.1.call-start = ((), (), s32[]{:S(2)}) async-start(), calls=%async_computation.9 | async-start | bytes 2621440 | tf_op jit(solution)/shard_map/reduce_scatter | solution.py:75
  314.9 106.5 %copy-start.2 = (bf16[512,2048]{1,0:T(8,128)(2,1)S(1)}, bf16[512,2048]{1,0:T(8,128)(2,1)}, u32[]{:S(2)}) copy-start(bf16[512,2048]{1,0:T(8,128)(2,1)} %get-tuple-element.6) | copy-start | bytes 6291460
  314.9 106.5 %copy-start.4 = (f32[2048]{0:T(1024)S(1)}, f32[2048]{0:T(1024)}, u32[]{:S(2)}) copy-start(f32[2048]{0:T(1024)} %param.19) | copy-start | bytes 24580
Sparse Core Ops, SparseCore 0:
  8.9 25.2 all-gather.9
  35.8 27.9 all-gather.15
  65.4 27.3 all-gather.13
  94.2 27.3 all-gather.11
  123.0 27.3 all-gather.17
  155.7 50.7 all-reduce.2
  208.1 106.7 all-gather.23
  316.5 104.9 all-gather.19
  423.0 104.9 all-gather.21
  541.4 29.4 reduce-scatter.1
